TPU v7x, 32 devices: a whole 2x2x4 slice. The times are simulated.
32 devices in a mesh: sp: 8 (over z, y), tp: 4 (over x, core).
Axes of the slice: x: 2, y: 2, z: 4, core: 2. Of those that a mesh axis runs over, the one named last changes fastest.
Arguments:
- residual_in: bfloat16 [3072, 2048], P(('sp', 'tp')), may hold values from -6 to 6
- queries: bfloat16 [3072, 2048], P('sp', 'tp'), may hold values from -180 to 180
- keys: bfloat16 [3072, 2048], P('sp', 'tp'), may hold values from -9 to 9
- values: bfloat16 [3072, 2048], P('sp', 'tp'), may hold values from -6 to 6
- mix_lambda: float32 [16], P('tp'), may hold values from 0.3 to 0.8
- head_gain: float32 [128], replicated, may hold values from 0.1 to 1.9
- out_weight: bfloat16 [2048, 2048], P('tp'), may hold values from -0.125 to 0.125
- norm_gain: float32 [2048], replicated, may hold values from 0.1 to 1.9
- gate_weight: bfloat16 [2048, 5632], P('sp', 'tp'), may hold values from -0.125 to 0.125
- up_weight: bfloat16 [2048, 5632], P('sp', 'tp'), may hold values from -0.125 to 0.125
- down_weight: bfloat16 [5632, 2048], P('tp', 'sp'), may hold values from -0.078125 to 0.078125
Outputs:
- layer_out: bfloat16 [3072, 2048], P(('sp', 'tp'))
All inputs are finite; a program needn't handle non-finite values.
Results may differ from a plain program's by a relative error of at most 0.014.
Values may be sent and summed in bfloat16 or wider, within the bound.
A program may use at most 128 MiB of HBM per device.

v0:
```python
import math

import jax
import jax.numpy as jnp
from jax import lax
from jax.sharding import PartitionSpec as P

DH = 64
VD = 128


def body(
    residual_in,
    queries,
    keys,
    values,
    mix_lambda,
    head_gain,
    out_weight,
    norm_gain,
    gate_weight,
    up_weight,
    down_weight,
):
    tp_count = lax.axis_size("tp")
    tok_local = queries.shape[0]
    heads_local = mix_lambda.shape[0]
    rows_local = tok_local // tp_count
    query_four = queries.reshape(tok_local, heads_local, 2, DH)
    inverse_root = 1.0 / math.sqrt(DH)

    def one_block(state, block):
        top, total, weighted = state
        key_block, value_block = block
        scores = (
            jnp.einsum("qhcd,khcd->hcqk", query_four, key_block, preferred_element_type=jnp.float32)
            * inverse_root
        )
        new_top = jnp.maximum(top, jnp.max(scores, axis=-1))
        rescale = jnp.exp(top - new_top)
        expo = jnp.exp(scores - new_top[..., None])
        total = total * rescale + jnp.sum(expo, axis=-1)
        weighted = weighted * rescale[..., None] + jnp.einsum(
            "hcqk,khe->hcqe",
            expo.astype(jnp.bfloat16),
            value_block,
            preferred_element_type=jnp.float32,
        )
        return ((new_top, total, weighted), None)

    start_state = (
        jnp.full((heads_local, 2, tok_local), -1e30, jnp.float32),
        jnp.zeros((heads_local, 2, tok_local), jnp.float32),
        jnp.zeros((heads_local, 2, tok_local, VD), jnp.float32),
    )
    key_piece = lax.all_gather(keys, "sp", axis=0, tiled=True)
    value_piece = lax.all_gather(values, "sp", axis=0, tiled=True)
    count = key_piece.shape[0]
    shards = max(count // tok_local, 1)
    unit = count // shards
    group = max(
        (g for g in range(1, shards + 1) if shards % g == 0 and g * unit <= max(1536, unit))
    )
    width = group * unit
    blocks = count // width
    key_blocks = key_piece.reshape(blocks, width, heads_local, 2, DH)
    value_blocks = value_piece.reshape(blocks, width, heads_local, VD)
    state, unused = lax.scan(one_block, start_state, (key_blocks, value_blocks))
    top, total, weighted = state
    maps = weighted / total[..., None]
    mixed = maps[:, 0] - mix_lambda[:, None, None] * maps[:, 1]
    head_scale = lax.rsqrt(jnp.mean(mixed * mixed, axis=-1, keepdims=True) + 1e-06)
    head_out = (mixed * head_scale * head_gain).astype(jnp.bfloat16)
    attended = jnp.transpose(head_out, (1, 0, 2)).reshape(tok_local, heads_local * VD)
    summed = lax.psum(
        jnp.dot(attended, out_weight, preferred_element_type=jnp.float32).astype(jnp.bfloat16), "tp"
    ).astype(jnp.float32)
    residual_all = lax.all_gather(residual_in, "tp", axis=0, tiled=True)
    after_all = residual_all.astype(jnp.float32) + summed
    row_scale = lax.rsqrt(jnp.mean(after_all * after_all, axis=-1, keepdims=True) + 1e-06)
    all_rows = (after_all * row_scale * norm_gain).astype(jnp.bfloat16)
    after_mix = lax.dynamic_slice_in_dim(
        after_all, lax.axis_index("tp") * rows_local, rows_local, 0
    )
    gate_all, up_all, down_all = (
        lax.all_gather(gate_weight, "sp", axis=0, tiled=True),
        lax.all_gather(up_weight, "sp", axis=0, tiled=True),
        lax.all_gather(down_weight, "sp", axis=1, tiled=True),
    )
    gate = jnp.dot(all_rows, gate_all, preferred_element_type=jnp.float32)
    up = jnp.dot(all_rows, up_all, preferred_element_type=jnp.float32)
    hidden = (jax.nn.silu(gate) * up).astype(jnp.bfloat16)
    mixer = lax.psum_scatter(
        jnp.dot(hidden, down_all, preferred_element_type=jnp.float32).astype(jnp.bfloat16),
        "tp",
        scatter_dimension=0,
        tiled=True,
    ).astype(jnp.float32)
    return (after_mix + 0.5 * mixer).astype(jnp.bfloat16)


def solution(mesh):
    return jax.shard_map(
        body,
        mesh=mesh,
        in_specs=(
            P(("sp", "tp"), None),
            P("sp", "tp"),
            P("sp", "tp"),
            P("sp", "tp"),
            P("tp"),
            P(),
            P("tp", None),
            P(),
            P("sp", "tp"),
            P("sp", "tp"),
            P("tp", "sp"),
        ),
        out_specs=P(("sp", "tp"), None),
        check_vma=False,
    )
```

profile of v0, /device:TPU:0, one launch (start us, length us, event | category | flops | bytes accessed | tf_op | source)
XLA Modules:
  0.0 579.6 jit_solution(15325134770839630398)
XLA Ops:
  6.5 0.7 all-gather.9.cloned.1.call-update
  7.3 0.7 all-gather.11.cloned.1.call-update
  8.8 1.2 copy.17
  10.0 62.3 %all-gather.9.cloned.1.call-done = bf16[3072,512]{1,0:T(8,128)(2,1)} async-done(((bf16[384,512]{1,0:T(8,128)(2,1)}), bf16[3072,512]{1,0:T(8,128)(2,1)}) %all-gather.9.cloned.1.call-update) | async-done | bytes 3145744 | tf_op jit(solution)/shard_map/all_gather | solution.py:56
  72.3 12.5 %reshape.39 = bf16[2,1536,4,2,64]{4,3,2,1,0:T(2,128)(2,1)} reshape(bf16[3072,512]{1,0:T(8,128)(2,1)} %all-gather.9.cloned.1.call-done) | data formatting | bytes 6291456 | tf_op jit(solution)/shard_map/reshape | solution.py:66
  84.8 15.4 %copy.18 = bf16[2,1536,4,2,64]{1,4,3,2,0:T(8,128)(2,1)} copy(bf16[2,1536,4,2,64]{4,3,2,1,0:T(2,128)(2,1)} %reshape.39) | data formatting | bytes 6291456
  100.2 33.0 %all-gather.11.cloned.1.call-done = bf16[3072,512]{1,0:T(8,128)(2,1)} async-done(((bf16[384,512]{1,0:T(8,128)(2,1)}), bf16[3072,512]{1,0:T(8,128)(2,1)}) %all-gather.11.cloned.1.call-update) | async-done | bytes 3145744 | tf_op jit(solution)/shard_map/all_gather | solution.py:57
  133.2 5.6 reshape.36
  138.7 63.8 %while.15 = (s32[]{:T(128)}, f32[4,2,384]{2,1,0:T(2,128)S(1)}, f32[4,2,384]{2,1,0:T(2,128)S(1)}, f32[4,2,384,128]{3,2,1,0:T(8,128)}, bf16[2,1536,4,2,64]{1,4,3,2...) while((s32[]{:T(128)}, f32[4,2,384]{2,1,0:T(2,128)S(1)}, ...), condition=%wide.region_3.4_spmd.clone, body=%wide.region_0.3_spmd.clone.sunk | while | flops 1850883072 | bytes 79233688 | solution.py:68
  138.7 10.6 %bitcast_reduce_fusion.2 = (f32[4,2,384]{2,1,0:T(2,128)S(1)}, f32[4,2,1536,384]{3,2,1,0:T(8,128)}) fusion(bf16[384,4,2,64]{0,3,2,1:T(8,128)(2,1)S(1)} %get-tuple-element.170, bf16[2,1536,4,2,64]{1,4,3,2,0:T(8,128)(2,1)} %get-tuple-element.169, s32[]{:T(128)} %get-tuple-element.156), kind=kOutput, calls=%fused_computation.1.clone.1 | convolution fusion | flops 613413888 | bytes 20853248 | tf_op jit(solution)/shard_map/while/body/eval_jaxpr/qhcd,khcd->hcqk/dot_general | solution.py:36
  149.4 9.5 %fusion.37 = f32[4,2,384]{2,1,0:T(2,128)S(1)} fusion(f32[4,2,1536,384]{3,2,1,0:T(8,128)} %get-tuple-element.144, f32[4,2,384]{2,1,0:T(2,128)S(1)} %fusion.36), kind=kLoop, calls=%fused_computation.4.clone.1 | loop fusion | flops 14152704 | bytes 18898944 | tf_op jit(solution)/shard_map/while/body/eval_jaxpr/reduce_sum | solution.py:42
  158.9 1.8 constant_dynamic-slice_fusion.2
  160.7 8.8 %fusion.39 = f32[4,2,384,128]{3,2,1,0:T(8,128)S(1)} fusion(f32[4,2,384,128]{3,2,1,0:T(8,128)S(1)} %copy-done.1, bf16[1,1536,4,128]{3,2,1,0:T(4,128)(2,1)S(1)} %constant_dynamic-slice_fusion.2, f32[4,2,1536,384]{3,2,1,0:T(8,128)} %get-tuple-element.144, f32[4,2,384]{2,1,0:T(2,128)S(1)} %fusion.36, f32[4,2,384]{2,1,0:T(2,128)S(1)} %get-tuple-element.146, ...), kind=kOutput, calls=%fused_computation.12.clone.1 | convolution fusion | flops 1223294976 | bytes 23617536 | tf_op jit(solution)/shard_map/while/body/eval_jaxpr/hcqk,khe->hcqe/dot_general | solution.py:43
  169.5 1.1 copy-done.2
  170.7 10.5 %bitcast_reduce_fusion.2 = (f32[4,2,384]{2,1,0:T(2,128)S(1)}, f32[4,2,1536,384]{3,2,1,0:T(8,128)}) fusion(bf16[384,4,2,64]{0,3,2,1:T(8,128)(2,1)S(1)} %get-tuple-element.170, bf16[2,1536,4,2,64]{1,4,3,2,0:T(8,128)(2,1)} %get-tuple-element.169, s32[]{:T(128)} %get-tuple-element.156), kind=kOutput, calls=%fused_computation.1.clone.1 | convolution fusion | flops 613413888 | bytes 20853248 | tf_op jit(solution)/shard_map/while/body/eval_jaxpr/qhcd,khcd->hcqk/dot_general | solution.py:36
  181.2 9.4 %fusion.37 = f32[4,2,384]{2,1,0:T(2,128)S(1)} fusion(f32[4,2,1536,384]{3,2,1,0:T(8,128)} %get-tuple-element.144, f32[4,2,384]{2,1,0:T(2,128)S(1)} %fusion.36), kind=kLoop, calls=%fused_computation.4.clone.1 | loop fusion | flops 14152704 | bytes 18898944 | tf_op jit(solution)/shard_map/while/body/eval_jaxpr/reduce_sum | solution.py:42
  190.7 1.8 constant_dynamic-slice_fusion.2
  192.6 8.8 %fusion.39 = f32[4,2,384,128]{3,2,1,0:T(8,128)S(1)} fusion(f32[4,2,384,128]{3,2,1,0:T(8,128)S(1)} %copy-done.1, bf16[1,1536,4,128]{3,2,1,0:T(4,128)(2,1)S(1)} %constant_dynamic-slice_fusion.2, f32[4,2,1536,384]{3,2,1,0:T(8,128)} %get-tuple-element.144, f32[4,2,384]{2,1,0:T(2,128)S(1)} %fusion.36, f32[4,2,384]{2,1,0:T(2,128)S(1)} %get-tuple-element.146, ...), kind=kOutput, calls=%fused_computation.12.clone.1 | convolution fusion | flops 1223294976 | bytes 23617536 | tf_op jit(solution)/shard_map/while/body/eval_jaxpr/hcqk,khe->hcqe/dot_general | solution.py:43
  201.4 1.1 copy-done.2
  202.5 3.1 copy.21
  205.6 1.5 broadcast_divide_fusion
  207.6 2.2 convolution_convert_fusion.1
  211.0 0.7 all-gather.17.cloned.1.call-update
  211.8 39.7 %all-reduce.2.cloned.1.call-done = bf16[384,2048]{1,0:T(8,128)(2,1)} async-done(((bf16[384,2048]{1,0:T(8,128)(2,1)}), bf16[384,2048]{1,0:T(8,128)(2,1)}) %all-reduce.2.cloned.1.call-update) | async-done | bytes 1572880 | tf_op jit(solution)/shard_map/psum | solution.py:75
  251.5 4.0 convert_add_fusion
  255.5 90.4 %all-gather.13.cloned.1.call-done = bf16[2048,1408]{1,0:T(8,128)(2,1)} async-done(((bf16[256,1408]{1,0:T(8,128)(2,1)}), bf16[2048,1408]{1,0:T(8,128)(2,1)}) %all-gather.13.cloned.1.call-update) | async-done | bytes 5767184 | tf_op jit(solution)/shard_map/all_gather | solution.py:86
  345.9 7.6 %fusion.21 = f32[384,1408]{1,0:T(8,128)} fusion(bf16[2048,1408]{1,0:T(8,128)(2,1)} %all-gather.13.cloned.1.call-done, f32[2048]{0:T(1024)S(1)} %copy-done.5, f32[384]{0:T(512)S(1)} %add_rsqrt_fusion.1, bf16[384,2048]{1,0:T(8,128)(2,1)} %all-reduce.2.cloned.1.call-done, bf16[384,2048]{1,0:T(8,128)(2,1)} %all-gather.7.cloned.1.call-done), kind=kOutput, calls=%fused_computation.40 | convolution fusion | flops 2219311104 | bytes 11085312 | tf_op jit(solution)/shard_map/dot_general | solution.py:90
  353.5 85.0 %all-gather.15.cloned.1.call-done = bf16[2048,1408]{1,0:T(8,128)(2,1)} async-done(((bf16[256,1408]{1,0:T(8,128)(2,1)}), bf16[2048,1408]{1,0:T(8,128)(2,1)}) %all-gather.15.cloned.1.call-update) | async-done | bytes 5767184 | tf_op jit(solution)/shard_map/all_gather | solution.py:87
  438.5 93.4 %all-gather.17.cloned.1.call-done = bf16[1408,2048]{1,0:T(8,128)(2,1)} async-done(((bf16[1408,256]{1,0:T(8,128)(2,1)}), bf16[1408,2048]{1,0:T(8,128)(2,1)}) %all-gather.17.cloned.1.call-update) | async-done | bytes 5767184 | tf_op jit(solution)/shard_map/all_gather | solution.py:88
  531.9 12.4 %convolution_convert_fusion = bf16[384,2048]{1,0:T(8,128)(2,1)} fusion(bf16[1408,2048]{1,0:T(8,128)(2,1)} %all-gather.17.cloned.1.call-done, bf16[2048,1408]{1,0:T(8,128)(2,1)} %all-gather.15.cloned.1.call-done, f32[384,1408]{1,0:T(8,128)} %fusion.21, f32[2048]{0:T(1024)S(1)} %copy-done.5, f32[384]{0:T(512)S(1)} %add_rsqrt_fusion.1, ...), kind=kOutput, calls=%fused_computation.27 | convolution fusion | flops 4437934080 | bytes 18425344 | tf_op jit(solution)/shard_map/dot_general | solution.py:94
  544.3 26.4 %reduce-scatter.2.cloned.1.call-done = bf16[96,2048]{1,0:T(8,128)(2,1)} async-done(((bf16[384,2048]{1,0:T(8,128)(2,1)}), bf16[96,2048]{1,0:T(8,128)(2,1)}) %reduce-scatter.2.cloned.1.call-update) | async-done | bytes 393232 | tf_op jit(solution)/shard_map/reduce_scatter | solution.py:93
  570.7 2.1 add_convert_fusion
  (42 shorter events, 2.6 us)
Async XLA Ops:
  6.5 201.0 %copy-start = (bf16[512,2048]{1,0:T(8,128)(2,1)S(1)}, bf16[512,2048]{1,0:T(8,128)(2,1)}, u32[]{:S(2)}) copy-start(bf16[512,2048]{1,0:T(8,128)(2,1)} %param.19) | copy-start | bytes 6291460
  6.5 65.8 %all-gather.9.cloned.1.call-start = ((), (), s32[]{:S(2)}) async-start(), calls=%async_computation.2 | async-start | bytes 3538944 | tf_op jit(solution)/shard_map/all_gather | solution.py:56
  7.3 125.9 %all-gather.11.cloned.1.call-start = ((), (), s32[]{:S(2)}) async-start(), calls=%async_computation.3 | async-start | bytes 3538944 | tf_op jit(solution)/shard_map/all_gather | solution.py:57
  8.0 203.8 %all-gather.7.cloned.1.call-start = ((), (), s32[]{:S(2)}) async-start(), calls=%async_computation.1 | async-start | bytes 1966080 | tf_op jit(solution)/shard_map/all_gather | solution.py:78
  8.7 242.7 %all-reduce.2.cloned.1.call-start = ((), (), s32[]{:S(2)}) async-start(), calls=%async_computation.4 | async-start | bytes 3145728 | tf_op jit(solution)/shard_map/psum | solution.py:75
  158.8 1.9 copy-start.1
  169.5 1.1 copy-start.2
  190.7 1.9 copy-start.1
  201.3 1.1 copy-start.2
  205.6 1.6 copy-start.3
  205.6 1.8 copy-start.4
  209.8 136.1 %all-gather.13.cloned.1.call-start = ((), (), s32[]{:S(2)}) async-start(), calls=%async_computation.5 | async-start | bytes 6488064 | tf_op jit(solution)/shard_map/all_gather | solution.py:86
  210.4 228.1 %all-gather.15.cloned.1.call-start = ((), (), s32[]{:S(2)}) async-start(), calls=%async_computation.6 | async-start | bytes 6488064 | tf_op jit(solution)/shard_map/all_gather | solution.py:87
  210.9 321.0 %all-gather.17.cloned.1.call-start = ((), (), s32[]{:S(2)}) async-start(), calls=%async_computation.7 | async-start | bytes 6488064 | tf_op jit(solution)/shard_map/all_gather | solution.py:88
  211.7 134.2 %copy-start.5 = (f32[2048]{0:T(1024)S(1)}, f32[2048]{0:T(1024)}, u32[]{:S(2)}) copy-start(f32[2048]{0:T(1024)} %param.20) | copy-start | bytes 24580
  211.7 359.0 %reduce-scatter.2.cloned.1.call-start = ((), (), s32[]{:S(2)}) async-start(), calls=%async_computation.8 | async-start | bytes 1966080 | tf_op jit(solution)/shard_map/reduce_scatter | solution.py:93
Sparse Core Ops, SparseCore 0:
  9.5 62.7 all-gather.8
  74.5 58.6 all-gather.10
  134.7 18.2 all-gather.6
  209.9 41.5 all-reduce.1
  253.5 92.3 all-gather.12
  347.9 90.5 all-gather.14
  440.5 91.2 all-gather.16
  544.4 26.2 reduce-scatter.1
where the time goes:
time: 581 us; the launch traced here: 580 us
  waiting for transfers between devices  434 us (75%)
  matrix products  60.9 us (10%)
  local copies, waits for them, and re-layouts  43.7 us (8%)
  other arithmetic  27.1 us (5%)
  between operations  13.6 us (2%)
    all_gather x1, waiting for transfers between devices, body(): lax.all_gather(down_weight, 'sp', axis=1, tiled=True)  93.4 us
    all_gather x1, waiting for transfers between devices, body(): lax.all_gather(gate_weight, 'sp', axis=0, tiled=True)  90.4 us
    all_gather x1, waiting for transfers between devices, body(): lax.all_gather(up_weight, 'sp', axis=0, tiled=True)  85 us
    all_gather x1, waiting for transfers between devices, body(): key_piece = lax.all_gather(keys, 'sp', axis=0, tiled=True)  62.3 us
    psum x1, waiting for transfers between devices, body(): lax.psum(jnp.dot(attended, out_weight, preferred_element_type=jnp.float32...  39.7 us
    all_gather x1, waiting for transfers between devices, body(): value_piece = lax.all_gather(values, 'sp', axis=0, tiled=True)  33 us
    reduce_scatter x1, waiting for transfers between devices, body(): lax.psum_scatter(jnp.dot(hidden, down_all, preferred_element_type=jnp.flo...  26.4 us
    dot_general x2, matrix products, one_block(): jnp.einsum('qhcd,khcd->hcqk', query_four, key_block, preferred_element_ty...  21.1 us
  transfers between devices with their start and end apart: 8, of which 7 were waited for; matrix products, arithmetic and copies ran while one was open for 20% of the time, Pallas kernels for 0%

commit v1 on v0

v1 whole, which is shorter than its diff:
```python
import functools
import math

import jax
import jax.numpy as jnp
from jax import lax
from jax.experimental import pallas as pl
from jax.experimental.pallas import tpu as pltpu
from jax.sharding import Mesh, PartitionSpec as P

DH = 64
VD = 128
LOG2E = 1.4426950408889634


def attention_kernel(heads, lam_ref, gain_ref, q_ref, k_ref, v_ref, o_ref, vx_ref):
    @pl.when(pl.program_id(0) == 0)
    def _():
        for h in range(heads):
            vx_ref[:, 2 * h * VD : (2 * h + 1) * VD] = v_ref[:, h * VD : (h + 1) * VD]
            vx_ref[:, (2 * h + 1) * VD : (2 * h + 2) * VD] = jnp.ones(
                (v_ref.shape[0], VD), jnp.bfloat16
            )

    scale = LOG2E / math.sqrt(DH)
    for h in range(heads):
        cols = slice(h * VD, (h + 1) * VD)
        q = q_ref[:, cols]
        lane = lax.broadcasted_iota(jnp.int32, q.shape, 1)
        maps = []
        for c in range(2):
            qc = jnp.where((lane >= DH) if c else (lane < DH), q, jnp.zeros_like(q))
            s = lax.dot_general(
                qc, k_ref[:, cols], (((1,), (1,)), ((), ())), preferred_element_type=jnp.float32
            )
            top = jnp.max(s, axis=-1, keepdims=True)
            e = jnp.exp2((s - top) * scale).astype(jnp.bfloat16)
            w = jnp.dot(
                e, vx_ref[:, 2 * h * VD : (2 * h + 2) * VD], preferred_element_type=jnp.float32
            )
            maps.append(w[:, :VD] / w[:, VD:])
        mixed = maps[0] - lam_ref[0:1, cols] * maps[1]
        norm = lax.rsqrt(jnp.mean(mixed * mixed, axis=-1, keepdims=True) + 1e-06)
        o_ref[:, cols] = (mixed * norm * gain_ref[...]).astype(jnp.bfloat16)


def attention(q, k, v, lam, gain):
    rows, width = q.shape
    heads = width // VD
    block = math.gcd(rows, 256)
    lam_wide = jnp.repeat(lam, VD).reshape(1, width)
    return pl.pallas_call(
        functools.partial(attention_kernel, heads),
        grid=(rows // block,),
        out_shape=jax.ShapeDtypeStruct((rows, width), jnp.bfloat16),
        in_specs=[
            pl.BlockSpec((1, width), lambda i: (0, 0)),
            pl.BlockSpec((1, VD), lambda i: (0, 0)),
            pl.BlockSpec((block, width), lambda i: (i, 0)),
            pl.BlockSpec(k.shape, lambda i: (0, 0)),
            pl.BlockSpec(v.shape, lambda i: (0, 0)),
        ],
        out_specs=pl.BlockSpec((block, width), lambda i: (i, 0)),
        scratch_shapes=[pltpu.VMEM((v.shape[0], 2 * width), jnp.bfloat16)],
        compiler_params=pltpu.CompilerParams(vmem_limit_bytes=60 * 1024 * 1024),
        cost_estimate=pl.CostEstimate(
            flops=rows * k.shape[0] * width * 8, bytes_accessed=4 * k.size * 2, transcendentals=0
        ),
    )(lam_wide, gain.reshape(1, VD), q, k, v)


def body(
    residual_in,
    queries,
    keys,
    values,
    mix_lambda,
    head_gain,
    out_weight,
    norm_gain,
    gate_weight,
    up_weight,
    down_weight,
):
    za, yb, tp = (lax.axis_size(name) for name in ("za", "yb", "tp"))
    tok_local, width = queries.shape
    rows, model = residual_in.shape
    heads = mix_lambda.shape[0] // za
    own = width // za

    def to_heads(a):
        return lax.all_to_all(a.reshape(tok_local, za, own), "za", 1, 0, tiled=False)

    qkv = jnp.stack(
        [a.reshape(tok_local, za, own).transpose(1, 0, 2) for a in (queries, keys, values)], 1
    )
    qkv = lax.all_to_all(qkv, "za", 0, 0, tiled=True)
    q = qkv[:, 0].reshape(za * tok_local, own)
    kv = lax.all_gather(qkv[:, 1:].transpose(1, 0, 2, 3), "yb", axis=1, tiled=True)
    k, v = kv[0].reshape(-1, own), kv[1].reshape(-1, own)

    lam = lax.dynamic_slice_in_dim(mix_lambda, lax.axis_index("za") * heads, heads, 0)
    out = attention(q, k, v, lam, head_gain)
    out = lax.all_to_all(
        out.reshape(za * tp, rows, own), ("za", "tp"), 0, 0, tiled=True
    )
    attended = (
        out.reshape(za, tp, rows, own).transpose(2, 1, 0, 3).reshape(rows, tp * width)
    )

    weights = jnp.stack([gate_weight.T, up_weight.T, down_weight])
    hid, depth = weights.shape[1] // za, weights.shape[2]
    weights = weights.reshape(3, za, hid, depth).transpose(1, 0, 2, 3)
    weights = lax.all_to_all(weights, "za", 0, 0, tiled=True)
    weights = lax.all_gather(weights, "yb", axis=0, tiled=False)
    weights = weights.transpose(2, 3, 1, 0, 4).reshape(3, hid, model)

    out_full = lax.all_gather(out_weight, "tp", axis=0, tiled=True)
    after = residual_in.astype(jnp.float32) + jnp.dot(
        attended, out_full, preferred_element_type=jnp.float32
    )
    row_scale = lax.rsqrt(jnp.mean(after * after, axis=-1, keepdims=True) + 1e-06)
    normed = (after * row_scale * norm_gain).astype(jnp.bfloat16)
    all_rows = lax.all_gather(normed, ("za", "tp"), axis=0, tiled=True)
    contract = (((1,), (1,)), ((), ()))
    gate = lax.dot_general(all_rows, weights[0], contract, preferred_element_type=jnp.float32)
    up = lax.dot_general(all_rows, weights[1], contract, preferred_element_type=jnp.float32)
    hidden = (jax.nn.silu(gate) * up).astype(jnp.bfloat16)
    mixer = lax.psum_scatter(
        jnp.dot(hidden, weights[2], preferred_element_type=jnp.float32).astype(jnp.bfloat16),
        ("za", "tp"),
        scatter_dimension=0,
        tiled=True,
    ).astype(jnp.float32)
    return (after + 0.5 * mixer).astype(jnp.bfloat16)


def solution(mesh):
    sp, tp = mesh.shape["sp"], mesh.shape["tp"]

    def run(*args):
        heads_local = args[4].shape[0] // tp
        za = math.gcd(heads_local, sp)
        cut = Mesh(mesh.devices.reshape(za, sp // za, tp), ("za", "yb", "tp"))
        s = ("za", "yb")
        return jax.shard_map(
            body,
            mesh=cut,
            in_specs=(
                P(("za", "yb", "tp"), None),
                P(s, "tp"),
                P(s, "tp"),
                P(s, "tp"),
                P("tp"),
                P(),
                P("tp", None),
                P(),
                P(s, "tp"),
                P(s, "tp"),
                P("tp", s),
            ),
            out_specs=P(("za", "yb", "tp"), None),
            check_vma=False,
        )(*args)

    return run
```

time: 581 us -> 368 us (0.63)
  waiting for transfers between devices: 434 us -> 168 us
  blocking collectives: 0 us -> 103 us
  matrix products: 60.9 us -> 24.4 us
  other arithmetic: 27.1 us -> 4.25 us
  Pallas kernels: 0 us -> 19.9 us
  local copies, waits for them, and re-layouts: 43.7 us -> 34.8 us
    all_gather x6 -> x4, waiting for transfers between devices: 364 us -> 83.1 us  [the longest x1 41.7 us: body(): weights = lax.all_gather(weights, 'yb', axis=0, tiled=False)]
    all_to_all x0 -> x3, blocking collectives: none -> 103 us  [the longest x1 52.1 us: body(): weights = lax.all_to_all(weights, 'za', 0, 0, tiled=True)]
    reduce_scatter x1, waiting for transfers between devices: 26.4 us -> 83.9 us  [body(): lax.psum_scatter(jnp.dot(hidden, weights[2], preferred_element_type=jnp.f...]
    psum x1 -> x0, waiting for transfers between devices: 39.7 us -> none  [body(): lax.psum(jnp.dot(attended, out_weight, preferred_element_type=jnp.float32...]
    dot_general x7 -> x3, matrix products: 60.9 us -> 24.4 us  [the longest x1 11.8 us: body(): jnp.dot(hidden, weights[2], preferred_element_type=jnp.float32)]
    pallas_call x0 -> x1, Pallas kernels: none -> 19.9 us  [attention(): pl.pallas_call(functools.partial(attention_kernel, heads), grid=(rows //...]
    reduce_sum x3 -> x0, other arithmetic: 19.1 us -> none  [the longest x2 18.9 us: one_block(): total = total * rescale + jnp.sum(expo, axis=-1)]
    reshape x2 -> x1, local copies, waits for them, and re-layouts: 18.1 us -> 0.29 us  [body(): out.reshape(za, tp, rows, own).transpose(2, 1, 0, 3)]
  transfers between devices with their start and end apart: 8 -> 5, of which waited for: 7 -> 3; matrix products, arithmetic and copies ran while one was open for 20% -> 10% of each run, Pallas kernels for 0% -> 5%
where the time goes in v1:
time: 368 us
  waiting for transfers between devices  168 us (46%)
  blocking collectives  103 us (28%)
  local copies, waits for them, and re-layouts  34.8 us (9%)
  matrix products  24.4 us (7%)
  Pallas kernels  19.9 us (5%)
  between operations  13.3 us (4%)
  other arithmetic  4.25 us (1%)
    reduce_scatter x1, waiting for transfers between devices, body(): lax.psum_scatter(jnp.dot(hidden, weights[2], preferred_element_type=jnp.f...  83.9 us
    all_to_all x1, blocking collectives, body(): weights = lax.all_to_all(weights, 'za', 0, 0, tiled=True)  52.1 us
    all_gather x1, waiting for transfers between devices, body(): weights = lax.all_gather(weights, 'yb', axis=0, tiled=False)  41.7 us
    all_gather x1, waiting for transfers between devices, body(): all_rows = lax.all_gather(normed, ('za', 'tp'), axis=0, tiled=True)  41.4 us
    all_to_all x1, blocking collectives, body(): qkv = lax.all_to_all(qkv, 'za', 0, 0, tiled=True)  34.7 us
    pallas_call x1, Pallas kernels, attention(): pl.pallas_call(functools.partial(attention_kernel, heads), grid=(rows //...  19.9 us
    all_to_all x1, blocking collectives, body(): lax.all_to_all(out.reshape(za * tp, rows, own), ('za', 'tp'), 0, 0, tiled...  16 us
    dot_general x1, matrix products, body(): jnp.dot(hidden, weights[2], preferred_element_type=jnp.float32)  11.8 us
  transfers between devices with their start and end apart: 5, of which 3 were waited for; matrix products, arithmetic and copies ran while one was open for 10% of the time, Pallas kernels for 5%

profile of v1, /device:TPU:0, one launch (start us, length us, event | category | flops | bytes accessed | tf_op | source)
XLA Modules:
  0.0 367.5 jit_solution(3400741004357093949)
XLA Ops:
  6.5 1.2 copy.44
  7.7 1.2 copy.45
  9.0 1.2 copy.46
  10.3 0.8 copy.47
  11.1 34.7 %all_to_all.15 = bf16[4,3,384,128]{3,2,1,0:T(8,128)(2,1)S(1)} all-to-all(bf16[4,3,384,128]{3,2,1,0:T(8,128)(2,1)S(1)} %copy.47), channel_id=1, replica_groups=mesh['za'=4,'yb'=2,'tp'=4] {'za'}, dimensions={0} | all-to-all | bytes 2359296 | tf_op jit(solution)/shard_map/all_to_all | solution.py:97
  45.8 0.9 slice_bitcast_fusion
  46.8 0.7 all-gather.8.cloned.1.call-update
  47.6 0.3 copy.49
  48.2 1.3 maximum_bitcast_fusion
  49.7 52.1 %all_to_all.16 = bf16[4,3,352,256]{3,2,1,0:T(8,128)(2,1)} all-to-all(bf16[4,3,352,256]{3,2,1,0:T(8,128)(2,1)S(1)} %copy.51), channel_id=1, replica_groups=mesh['za'=4,'yb'=2,'tp'=4] {'za'}, dimensions={0} | all-to-all | bytes 4325376 | tf_op jit(solution)/shard_map/all_to_all | solution.py:114
  101.9 0.6 copy-done.6
  102.5 0.6 dynamic_slice.5
  103.1 0.8 slice.31
  103.9 2.8 fusion.3
  106.7 1.2 broadcast_in_dim.2.lam_ref
  107.8 19.9 %shard_map.109 = bf16[1536,128]{1,0:T(8,128)(2,1)} custom-call(f32[1,128]{1,0:T(1,128)} %broadcast_in_dim.2.lam_ref, f32[1,128]{1,0:T(1,128)} %bitcast.59, bf16[1536,128]{1,0:T(8,128)(2,1)} %bitcast.57, bf16[3072,128]{1,0:T(8,128)(2,1)} %bitcast.55, bf16[3072,128]{1,0:T(8,128)(2,1)} %bitcast.54), custom_call_target="tpu_custom_call" | custom-call | flops 4831838208 | bytes 3145728 | tf_op jit(solution)/shard_map/pallas_call | solution.py:52
  127.7 16.0 %all_to_all.17 = bf16[16,96,128]{2,1,0:T(8,128)(2,1)S(1)} all-to-all(bf16[16,96,128]{2,1,0:T(8,128)(2,1)} %bitcast.58), channel_id=1, replica_groups=mesh['za'=4,'yb'=2,'tp'=4] {'za','tp'}, dimensions={0} | all-to-all | bytes 786432 | tf_op jit(solution)/shard_map/all_to_all | solution.py:104
  143.7 0.3 copy.48
  144.0 0.3 reshape.51
  144.3 5.6 %multiply_reduce_fusion = (f32[96]{0:T(128)S(1)}, f32[96,2048]{1,0:T(8,128)S(1)}) fusion(bf16[96,2048]{1,0:T(8,128)(2,1)S(1)} %reshape.51, bf16[2048,2048]{1,0:T(8,128)(2,1)} %all-gather.8.cloned.1.call-done, bf16[96,2048]{1,0:T(8,128)(2,1)S(1)} %copy-done.4), kind=kOutput, calls=%fused_computation.10 | convolution fusion | flops 806092672 | bytes 9961856 | tf_op jit(solution)/shard_map/dot_general | solution.py:119
  150.0 0.9 multiply_convert_fusion
  151.1 41.7 %all-gather.12.cloned.1.call-done = bf16[8,3,352,256]{3,2,1,0:T(8,128)(2,1)} async-done(((bf16[4,3,352,256]{3,2,1,0:T(8,128)(2,1)}), bf16[8,3,352,256]{3,2,1,0:T(8,128)(2,1)}) %all-gather.12.cloned.1.call-update) | async-done | bytes 4325392 | tf_op jit(solution)/shard_map/all_gather | solution.py:115
  192.9 6.7 %copy.54 = bf16[2,4,3,352,256]{4,0,1,3,2:T(2,128)(2,1)S(1)} copy(bf16[2,4,3,352,256]{4,3,2,1,0:T(8,128)(2,1)} %bitcast.47) | data formatting | bytes 8650752 | tf_op jit(solution)/shard_map/all_gather | solution.py:115
  199.5 4.2 %fusion.2 = (bf16[1,352,4,2,256]{4,3,2,1,0:T(2,128)(2,1)}, bf16[1,352,4,2,256]{4,3,2,1,0:T(2,128)(2,1)}, bf16[1,352,4,2,256]{4,3,2,1,0:T(2,128)(2,1)}) fusion(bf16[3,352,4,2,256]{4,3,2,1,0:T(2,128)(2,1)S(1)} %bitcast.46), kind=kLoop, calls=%fused_computation.13 | loop fusion | bytes 8650752 | tf_op jit(solution)/shard_map/slice | solution.py:126
  203.8 4.6 %squeeze.9 = bf16[352,2048]{1,0:T(8,128)(2,1)} reshape(bf16[1,352,4,2,256]{4,3,2,1,0:T(2,128)(2,1)} %get-tuple-element.5) | data formatting | bytes 2883584 | tf_op jit(solution)/shard_map/squeeze | solution.py:126
  208.3 4.7 %squeeze.11 = bf16[352,2048]{1,0:T(8,128)(2,1)} reshape(bf16[1,352,4,2,256]{4,3,2,1,0:T(2,128)(2,1)} %get-tuple-element.6) | data formatting | bytes 2883584 | tf_op jit(solution)/shard_map/squeeze | solution.py:130
  213.1 2.0 squeeze.10
  215.0 41.4 %all-gather.10.cloned.1.call-done = bf16[1536,2048]{1,0:T(8,128)(2,1)} async-done(((bf16[96,2048]{1,0:T(8,128)(2,1)}), bf16[1536,2048]{1,0:T(8,128)(2,1)}) %all-gather.10.cloned.1.call-update) | async-done | bytes 6291472 | tf_op jit(solution)/shard_map/all_gather | solution.py:124
  256.4 7.0 %fusion.4 = f32[1536,352]{0,1:T(8,128)} fusion(bf16[1536,2048]{1,0:T(8,128)(2,1)} %all-gather.10.cloned.1.call-done, bf16[352,2048]{1,0:T(8,128)(2,1)} %squeeze.9), kind=kOutput, calls=%fused_computation.15 | convolution fusion | flops 2214592512 | bytes 9895936 | tf_op jit(solution)/shard_map/dot_general | solution.py:126
  263.4 11.8 %convolution_convert_fusion = bf16[1536,2048]{1,0:T(8,128)(2,1)} fusion(bf16[352,2048]{1,0:T(8,128)(2,1)S(1)} %copy-done.1, bf16[1536,2048]{1,0:T(8,128)(2,1)} %all-gather.10.cloned.1.call-done, bf16[352,2048]{1,0:T(8,128)(2,1)} %squeeze.10, f32[1536,352]{0,1:T(8,128)} %fusion.4), kind=kOutput, calls=%fused_computation | convolution fusion | flops 4435574784 | bytes 17629184 | tf_op jit(solution)/shard_map/dot_general | solution.py:130
  275.2 83.9 %reduce-scatter.2.cloned.1.call-done = bf16[96,2048]{1,0:T(8,128)(2,1)} async-done(((bf16[1536,2048]{1,0:T(8,128)(2,1)}), bf16[96,2048]{1,0:T(8,128)(2,1)}) %reduce-scatter.2.cloned.1.call-update) | async-done | bytes 393232 | tf_op jit(solution)/shard_map/reduce_scatter | solution.py:129
  359.1 1.9 add_convert_fusion
  (28 shorter events, 1.1 us)
Async XLA Ops:
  6.5 97.3 %all-gather.6.cloned.1.call-start = ((), (), s32[]{:S(2)}) async-start(), calls=%async_computation.4 | async-start | bytes 2359296 | tf_op jit(solution)/shard_map/all_gather | solution.py:99
  45.8 1.8 copy-start.2
  46.7 1.2 copy-start.3
  46.8 97.5 %all-gather.8.cloned.1.call-start = ((), (), s32[]{:S(2)}) async-start(), calls=%async_computation.5 | async-start | bytes 10485760 | tf_op jit(solution)/shard_map/all_gather | solution.py:118
  47.5 145.3 %all-gather.12.cloned.1.call-start = ((), (), s32[]{:S(2)}) async-start(), calls=%async_computation.8 | async-start | bytes 6488064 | tf_op jit(solution)/shard_map/all_gather | solution.py:115
  101.8 0.7 copy-start.6
  101.8 154.6 %all-gather.10.cloned.1.call-start = ((), (), s32[]{:S(2)}) async-start(), calls=%async_computation.6 | async-start | bytes 6684672 | tf_op jit(solution)/shard_map/all_gather | solution.py:124
  127.7 16.6 %copy-start.4 = (bf16[96,2048]{1,0:T(8,128)(2,1)S(1)}, bf16[96,2048]{1,0:T(8,128)(2,1)}, u32[]{:S(2)}) copy-start(bf16[96,2048]{1,0:T(8,128)(2,1)} %param.11) | copy-start | bytes 1179652
  144.3 5.7 %copy-start.5 = (f32[2048]{0:T(1024)S(1)}, f32[2048]{0:T(1024)}, u32[]{:S(2)}) copy-start(f32[2048]{0:T(1024)} %param.18) | copy-start | bytes 24580
  150.9 208.2 %reduce-scatter.2.cloned.1.call-start = ((), (), s32[]{:S(2)}) async-start(), calls=%async_computation.7 | async-start | bytes 6684672 | tf_op jit(solution)/shard_map/reduce_scatter | solution.py:129
  208.3 4.7 %copy-start = (bf16[1,352,4,2,256]{4,3,2,1,0:T(2,128)(2,1)S(1)}, bf16[1,352,4,2,256]{4,3,2,1,0:T(2,128)(2,1)}, u32[]{:S(2)}) copy-start(bf16[1,352,4,2,256]{4,3,2,1,0:T(2,128)(2,1)} %get-tuple-element.7) | copy-start | bytes 4325380
  215.0 48.3 %copy-start.1 = (bf16[352,2048]{1,0:T(8,128)(2,1)S(1)}, bf16[352,2048]{1,0:T(8,128)(2,1)}, u32[]{:S(2)}) copy-start(bf16[352,2048]{1,0:T(8,128)(2,1)} %squeeze.11) | copy-start | bytes 4325380
Sparse Core Ops, SparseCore 0:
  46.9 26.2 all-gather.5
  74.8 58.2 all-gather.7
  134.6 58.1 all-gather.11
  195.0 61.3 all-gather.9
  275.3 83.7 reduce-scatter.1

commit v2 on v1

v2 whole, which is shorter than its diff:
```python
import functools
import math

import jax
import jax.numpy as jnp
from jax import lax
from jax.experimental import pallas as pl
from jax.experimental.pallas import tpu as pltpu
from jax.sharding import Mesh, PartitionSpec as P

DH = 64
VD = 128
LOG2E = 1.4426950408889634


MESH = pl.DeviceIdType.MESH
AXES = ("za", "yb", "tp")


def remote(src, dst, send, recv, **where):
    return pltpu.make_async_remote_copy(
        src_ref=src, dst_ref=dst, send_sem=send, recv_sem=recv, device_id=where, device_id_type=MESH
    )


def front_kernel(n, lam_ref, gain_ref, qkv, w, o_out, w_out, scr, kk, vx, osend,
                 q_s, q_r, y_s, y_r, w_s, w_r, wy_s, wy_r, o_s, o_r, l_s):
    nz, ny, nt, heads, aligned = n
    z, y, t = (lax.axis_index(name) for name in AXES)
    tok, rows = scr.shape[3], osend.shape[1]
    depth = w.shape[2]

    def place(zz, yy):
        at = zz * ny + yy
        return w_out.at[:, pl.ds(pl.multiple_of(at * depth, depth), depth)] if aligned else w_out.at[at]

    barrier = pltpu.get_barrier_semaphore()
    me = z * nt + t
    for i in range(1, nz * nt):
        p = lax.rem(me + i, nz * nt)
        pl.semaphore_signal(barrier, inc=1, device_id={"za": p // nt, "tp": lax.rem(p, nt)}, device_id_type=MESH)
    for f in range(1, ny):
        pl.semaphore_signal(barrier, inc=1, device_id={"yb": lax.rem(y + f, ny)}, device_id_type=MESH)
    pl.semaphore_wait(barrier, nz * nt - 1 + ny - 1)

    def q_copy(d):
        zp = lax.rem(z + d, nz)
        return remote(qkv.at[zp], scr.at[z, y], q_s.at[d], q_r.at[z], za=zp)

    def kv_own(f):
        return remote(qkv.at[z, pl.ds(1, 2)], scr.at[z, y, pl.ds(1, 2)], y_s.at[0, f], y_r.at[z, y],
                      yb=lax.rem(y + f, ny))

    def kv_copy(d, f):
        zp = lax.rem(z + d, nz)
        part = scr.at[zp, y, pl.ds(1, 2)]
        return remote(part, part, y_s.at[d, f], y_r.at[zp, y], yb=lax.rem(y + f, ny))

    def w_copy(d):
        zp = lax.rem(z + d, nz)
        return remote(w.at[zp], place(z, y), w_s.at[d], w_r.at[z], za=zp)

    def w_own(f):
        return remote(w.at[z], place(z, y), wy_s.at[0, f], wy_r.at[z, y], yb=lax.rem(y + f, ny))

    def w_pass(d, f):
        zp = lax.rem(z + d, nz)
        return remote(place(zp, y), place(zp, y), wy_s.at[d, f], wy_r.at[zp, y], yb=lax.rem(y + f, ny))

    for d in range(1, nz):
        q_copy(d).start()
    for f in range(1, ny):
        kv_own(f).start()
    local = pltpu.make_async_copy(w.at[z], place(z, y), l_s)
    local.start()
    for d in range(1, nz):
        w_copy(d).start()
    for f in range(1, ny):
        w_own(f).start()
    scr[z, y] = qkv[z]
    for d in range(1, nz):
        zp = lax.rem(z + d, nz)
        remote(qkv.at[z], scr.at[zp, y], q_s.at[d], q_r.at[zp], za=zp).wait_recv()
        for f in range(1, ny):
            kv_copy(d, f).start()
    for d in range(nz):
        zp = lax.rem(z + d, nz)
        for f in range(1, ny):
            yp = lax.rem(y + f, ny)
            part = scr.at[zp, yp, pl.ds(1, 2)]
            remote(part, part, y_s.at[d, f], y_r.at[zp, yp], yb=yp).wait_recv()
    for zz in range(nz):
        for yy in range(ny):
            span = slice((zz * ny + yy) * tok, (zz * ny + yy + 1) * tok)
            kk[span] = scr[zz, yy, 1]
            for h in range(heads):
                vx[span, 2 * h * VD : (2 * h + 1) * VD] = scr[zz, yy, 2, :, h * VD : (h + 1) * VD]
                vx[span, (2 * h + 1) * VD : (2 * h + 2) * VD] = jnp.ones((tok, VD), jnp.bfloat16)

    scale = LOG2E / math.sqrt(DH)

    def o_copy(p):
        return remote(osend.at[p], o_out.at[me], o_s.at[p], o_r.at[me], za=p // nt, tp=lax.rem(p, nt))

    def block(i, carry):
        zq = i // (nt // 2)
        off = lax.rem(i, nt // 2) * (2 * rows)
        for h in range(heads):
            cols = slice(h * VD, (h + 1) * VD)
            q = scr[zq, y, 0, pl.ds(pl.multiple_of(off, 2 * rows), 2 * rows), cols]
            lane = lax.broadcasted_iota(jnp.int32, q.shape, 1)
            maps = []
            for c in range(2):
                qc = jnp.where((lane >= DH) if c else (lane < DH), q, jnp.zeros_like(q))
                s = lax.dot_general(
                    qc, kk[:, cols], (((1,), (1,)), ((), ())), preferred_element_type=jnp.float32
                )
                top = jnp.max(s, axis=-1, keepdims=True)
                e = jnp.exp2((s - top) * scale).astype(jnp.bfloat16)
                o = jnp.dot(
                    e, vx[:, 2 * h * VD : (2 * h + 2) * VD], preferred_element_type=jnp.float32
                )
                maps.append(o[:, :VD] / o[:, VD:])
            mixed = maps[0] - lam_ref[0:1, cols] * maps[1]
            norm = lax.rsqrt(jnp.mean(mixed * mixed, axis=-1, keepdims=True) + 1e-06)
            done = (mixed * norm * gain_ref[...]).astype(jnp.bfloat16)
            osend[2 * i, :, cols] = done[:rows]
            osend[2 * i + 1, :, cols] = done[rows:]
        for j in range(2):
            p = 2 * i + j

            @pl.when(p != me)
            def _():
                o_copy(p).start()

        return carry

    lax.fori_loop(0, nz * nt // 2, block, 0)
    o_out[me] = osend[me]
    for d in range(1, nz):
        zp = lax.rem(z + d, nz)
        remote(w.at[z], place(zp, y), w_s.at[d], w_r.at[zp], za=zp).wait_recv()
        if d == 1:
            local.wait()
        for f in range(1, ny):
            w_pass(d, f).start()
    for i in range(1, nz * nt):
        p = lax.rem(me + i, nz * nt)
        remote(osend.at[p], o_out.at[p], o_s.at[p], o_r.at[p], za=p // nt, tp=lax.rem(p, nt)).wait_recv()
        o_copy(p).wait_send()
    for d in range(nz):
        zp = lax.rem(z + d, nz)
        for f in range(1, ny):
            yp = lax.rem(y + f, ny)
            remote(place(zp, yp), place(zp, yp), wy_s.at[d, f], wy_r.at[zp, yp], yb=yp).wait_recv()
            if d:
                w_pass(d, f).wait_send()
                kv_copy(d, f).wait_send()
            else:
                w_own(f).wait_send()
                kv_own(f).wait_send()
        if d:
            q_copy(d).wait_send()
            w_copy(d).wait_send()


def front(qkv, weights, lam, gain, rows, sizes):
    nz, ny, nt, heads = sizes
    tok, own = qkv.shape[2:]
    hid, depth = weights.shape[1:]
    aligned = depth % 128 == 0
    w_shape = (hid, nz * ny * depth) if aligned else (nz * ny, hid, depth)
    vmem = pl.BlockSpec(memory_space=pltpu.VMEM)
    dma = pltpu.SemaphoreType.DMA
    out, gathered = pl.pallas_call(
        functools.partial(front_kernel, (nz, ny, nt, heads, aligned)),
        out_shape=(
            jax.ShapeDtypeStruct((nz * nt, rows, own), jnp.bfloat16),
            jax.ShapeDtypeStruct(w_shape, jnp.bfloat16),
        ),
        in_specs=[vmem, vmem, vmem, pl.BlockSpec(memory_space=pl.ANY)],
        out_specs=(vmem, pl.BlockSpec(memory_space=pl.ANY)),
        scratch_shapes=[
            pltpu.VMEM((nz, ny, 3, tok, own), jnp.bfloat16),
            pltpu.VMEM((nz * ny * tok, own), jnp.bfloat16),
            pltpu.VMEM((nz * ny * tok, 2 * own), jnp.bfloat16),
            pltpu.VMEM((nz * nt, rows, own), jnp.bfloat16),
            dma((nz,)), dma((nz,)),
            dma((nz, ny)), dma((nz, ny)),
            dma((nz,)), dma((nz,)),
            dma((nz, ny)), dma((nz, ny)),
            dma((nz * nt,)), dma((nz * nt,)),
            dma,
        ],
        compiler_params=pltpu.CompilerParams(
            collective_id=1, has_side_effects=True, vmem_limit_bytes=60 * 1024 * 1024
        ),
        cost_estimate=pl.CostEstimate(
            flops=100_000_000_000, bytes_accessed=20_000_000, transcendentals=0
        ),
    )(jnp.repeat(lam, VD).reshape(1, own), gain.reshape(1, VD), qkv, weights)
    if not aligned:
        gathered = gathered.transpose(1, 0, 2).reshape(hid, nz * ny * depth)
    return out, gathered


def mixer_kernel(n, normed, after, w, out, got, mine, c_send, c_recv, x_send, x_recv, z_send, z_recv,
                 az_s, az_r, ax_s, ax_r, ac_s, ac_r, rc_s, rc_r, rx_s, rx_r, rz_s, rz_r):
    nz, nx = n
    z, y, t = (lax.axis_index(name) for name in AXES)
    x, c = t // 2, lax.rem(t, 2)
    other = 1 - c
    rows, model = normed.shape
    hid = w.shape[0] // 3

    barrier = pltpu.get_barrier_semaphore()
    for d in range(1, nz):
        pl.semaphore_signal(barrier, inc=1, device_id={"za": lax.rem(z + d, nz)}, device_id_type=MESH)
    for e in range(1, nx):
        pl.semaphore_signal(barrier, inc=1, device_id={"tp": lax.rem(x + e, nx) * 2 + c}, device_id_type=MESH)
    pl.semaphore_signal(barrier, inc=1, device_id={"tp": x * 2 + other}, device_id_type=MESH)
    pl.semaphore_wait(barrier, nz + nx - 1)

    def at(d, e):
        return lax.rem(z + d, nz), lax.rem(x + e, nx)

    def slot(d, e, cc):
        zp, xp = at(d, e)
        return got.at[zp, xp, pl.ds(pl.multiple_of(cc * rows, rows), rows)]

    def ag_z(d):
        return remote(normed, slot(0, 0, c), az_s.at[d], az_r.at[z], za=lax.rem(z + d, nz))

    def ag_x(d, e):
        src = slot(d, 0, c) if d else normed
        return remote(src, slot(d, 0, c), ax_s.at[d, e], ax_r.at[lax.rem(z + d, nz), x],
                      tp=lax.rem(x + e, nx) * 2 + c)

    def ag_c(d, e):
        zp, xp = at(d, e)
        src = slot(d, e, c) if (d or e) else normed
        return remote(src, slot(d, e, c), ac_s.at[d, e], ac_r.at[zp, xp], tp=x * 2 + other)

    def rs_c(d, e):
        return remote(c_send.at[d, e], c_recv.at[d, e], rc_s.at[d, e], rc_r.at[d, e], tp=x * 2 + other)

    def rs_x(d, e):
        return remote(x_send.at[d, e], x_recv.at[d, e], rx_s.at[d, e], rx_r.at[d, e],
                      tp=lax.rem(x + e, nx) * 2 + c)

    def rs_z(d):
        return remote(z_send.at[d], z_recv.at[d], rz_s.at[d], rz_r.at[d], za=lax.rem(z + d, nz))

    for d in range(1, nz):
        ag_z(d).start()
    for e in range(1, nx):
        ag_x(0, e).start()
    ag_c(0, 0).start()
    got[z, x, pl.ds(pl.multiple_of(c * rows, rows), rows)] = normed[...]

    def after_core(d, e):
        rs_c(d, e).wait_recv()
        both = mine[d, e].astype(jnp.float32) + c_recv[d, e].astype(jnp.float32)
        if e:
            x_send[d, e] = both.astype(jnp.bfloat16)
            rs_x(d, e).start()
        else:
            mine[d, e] = both

    def after_x(d):
        total = mine[d, 0]
        for e in range(1, nx):
            rs_x(d, e).wait_recv()
            total = total + x_recv[d, e].astype(jnp.float32)
        if d:
            z_send[d] = total.astype(jnp.bfloat16)
            rs_z(d).start()
        else:
            mine[0, 0] = total

    steps = [(d, e) for d in range(nz) for e in range(nx)]
    contract = (((1,), (1,)), ((), ()))
    for k, (d, e) in enumerate(steps):
        zp, xp = at(d, e)
        if d and e == 0:
            remote(normed, slot(d, 0, c), az_s.at[d], az_r.at[zp], za=zp).wait_recv()
            for f in range(1, nx):
                ag_x(d, f).start()
            ag_c(d, 0).start()
        if e:
            remote(normed, slot(d, e, c), ax_s.at[d, e], ax_r.at[zp, xp], tp=xp * 2 + c).wait_recv()
            ag_c(d, e).start()
        remote(normed, slot(d, e, other), ac_s.at[d, e], ac_r.at[zp, xp], tp=x * 2 + other).wait_recv()
        block = got[zp, xp]
        gate = lax.dot_general(block, w[0:hid], contract, preferred_element_type=jnp.float32)
        up = lax.dot_general(block, w[hid : 2 * hid], contract, preferred_element_type=jnp.float32)
        hidden = (jax.nn.silu(gate) * up).astype(jnp.bfloat16)
        part = jnp.dot(hidden, w[2 * hid :], preferred_element_type=jnp.float32)
        low, high = part[:rows], part[rows:]
        mine[d, e] = jnp.where(c == 0, low, high)
        c_send[d, e] = jnp.where(c == 0, high, low).astype(jnp.bfloat16)
        rs_c(d, e).start()
        if k:
            after_core(*steps[k - 1])
        if d and e == nx - 1:
            after_x(d - 1)
    after_core(*steps[-1])
    after_x(nz - 1)
    total = mine[0, 0]
    for d in range(1, nz):
        rs_z(d).wait_recv()
        total = total + z_recv[d].astype(jnp.float32)
    out[...] = (after[...] + 0.5 * total).astype(jnp.bfloat16)
    for d, e in steps:
        ag_c(d, e).wait_send()
        rs_c(d, e).wait_send()
        if e:
            ag_x(d, e).wait_send()
            rs_x(d, e).wait_send()
        elif d:
            ag_z(d).wait_send()
            rs_z(d).wait_send()


def mixer_call(normed, after, weights, sizes):
    nz, nx = sizes
    rows, model = normed.shape
    dma = pltpu.SemaphoreType.DMA
    vmem = pl.BlockSpec(memory_space=pltpu.VMEM)
    half = (nz, nx, rows, model)
    return pl.pallas_call(
        functools.partial(mixer_kernel, sizes),
        out_shape=jax.ShapeDtypeStruct((rows, model), jnp.bfloat16),
        in_specs=[vmem] * 3,
        out_specs=vmem,
        scratch_shapes=[
            pltpu.VMEM((nz, nx, 2 * rows, model), jnp.bfloat16),
            pltpu.VMEM(half, jnp.float32),
            pltpu.VMEM(half, jnp.bfloat16),
            pltpu.VMEM(half, jnp.bfloat16),
            pltpu.VMEM(half, jnp.bfloat16),
            pltpu.VMEM(half, jnp.bfloat16),
            pltpu.VMEM((nz, rows, model), jnp.bfloat16),
            pltpu.VMEM((nz, rows, model), jnp.bfloat16),
            dma((nz,)), dma((nz,)),
            dma((nz, nx)), dma((nz, nx)),
            dma((nz, nx)), dma((nz, nx)),
            dma((nz, nx)), dma((nz, nx)),
            dma((nz, nx)), dma((nz, nx)),
            dma((nz,)), dma((nz,)),
        ],
        compiler_params=pltpu.CompilerParams(
            collective_id=2, has_side_effects=True, vmem_limit_bytes=62 * 1024 * 1024
        ),
        cost_estimate=pl.CostEstimate(
            flops=100_000_000_000, bytes_accessed=20_000_000, transcendentals=0
        ),
    )(normed, after, weights)


def body(
    residual_in,
    queries,
    keys,
    values,
    mix_lambda,
    head_gain,
    out_weight,
    norm_gain,
    gate_weight,
    up_weight,
    down_weight,
):
    za, yb, tp = (lax.axis_size(name) for name in AXES)
    tok_local, width = queries.shape
    rows, model = residual_in.shape
    heads = mix_lambda.shape[0] // za
    own = width // za

    out_full = lax.all_gather(out_weight, "tp", axis=0, tiled=True)
    qkv = jnp.stack(
        [a.reshape(tok_local, za, own).transpose(1, 0, 2) for a in (queries, keys, values)], 1
    )
    hid = down_weight.shape[0] // za
    weights = jnp.stack(
        [a.reshape(za, hid, -1) for a in (gate_weight.T, up_weight.T, down_weight)], 1
    ).reshape(za, 3 * hid, -1)
    lam = lax.dynamic_slice_in_dim(mix_lambda, lax.axis_index("za") * heads, heads, 0)
    out, weights = front(qkv, weights, lam, head_gain, rows, (za, yb, tp, heads))
    attended = (
        out.reshape(za, tp, rows, own).transpose(2, 1, 0, 3).reshape(rows, tp * width)
    )
    after = residual_in.astype(jnp.float32) + jnp.dot(
        attended, out_full, preferred_element_type=jnp.float32
    )
    row_scale = lax.rsqrt(jnp.mean(after * after, axis=-1, keepdims=True) + 1e-06)
    normed = (after * row_scale * norm_gain).astype(jnp.bfloat16)
    return mixer_call(normed, after, weights, (za, tp // 2))


def solution(mesh):
    sp, tp = mesh.shape["sp"], mesh.shape["tp"]

    def run(*args):
        heads_local = args[4].shape[0] // tp
        za = math.gcd(heads_local, sp)
        cut = Mesh(mesh.devices.reshape(za, sp // za, tp), ("za", "yb", "tp"))
        s = ("za", "yb")
        return jax.shard_map(
            body,
            mesh=cut,
            in_specs=(
                P(("za", "yb", "tp"), None),
                P(s, "tp"),
                P(s, "tp"),
                P(s, "tp"),
                P("tp"),
                P(),
                P("tp", None),
                P(),
                P(s, "tp"),
                P(s, "tp"),
                P("tp", s),
            ),
            out_specs=P(("za", "yb", "tp"), None),
            check_vma=False,
        )(*args)

    return run
```

time: 368 us -> 267 us (0.73)
  Pallas kernels: 19.9 us -> 236 us
  waiting for transfers between devices: 168 us -> 0.73 us
  blocking collectives: 103 us -> 0 us
  local copies, waits for them, and re-layouts: 34.8 us -> 9.03 us
  matrix products: 24.4 us -> 4.98 us
    pallas_call x1 -> x2, Pallas kernels: 19.9 us -> 236 us  [the longest x1 136 us: mixer_call(): pl.pallas_call(functools.partial(mixer_kernel, sizes), out_shape=jax.Shap...]
    all_to_all x3 -> x0, blocking collectives: 103 us -> none  [the longest x1 52.1 us: body(): weights = lax.all_to_all(weights, 'za', 0, 0, tiled=True)]
    reduce_scatter x1 -> x0, waiting for transfers between devices: 83.9 us -> none  [body(): lax.psum_scatter(jnp.dot(hidden, weights[2], preferred_element_type=jnp.f...]
    all_gather x3 -> x0, waiting for transfers between devices: 83.1 us -> none  [the longest x1 41.7 us: body(): weights = lax.all_gather(weights, 'yb', axis=0, tiled=False)]
    dot_general x2 -> x0, matrix products: 18.8 us -> none  [the longest x1 11.8 us: body(): jnp.dot(hidden, weights[2], preferred_element_type=jnp.float32)]
    squeeze x3 -> x0, local copies, waits for them, and re-layouts: 11.3 us -> none  [the longest x1 4.72 us: body(): weights[2]]
    slice x3 -> x0, local copies, waits for them, and re-layouts: 7.78 us -> none  [the longest x1 4.24 us: body(): weights[0]]
    all_gather x1 -> x0, local copies, waits for them, and re-layouts: 6.67 us -> none  [body(): weights = lax.all_gather(weights, 'yb', axis=0, tiled=False)]
  transfers between devices with their start and end apart: 5 -> 1, of which waited for: 3 -> 0; matrix products, arithmetic and copies ran while one was open for 10% -> 3% of each run, Pallas kernels for 5% -> 38%
where the time goes in v2:
time: 267 us
  Pallas kernels  236 us (88%)
  between operations  13.6 us (5%)
  local copies, waits for them, and re-layouts  9.03 us (3%)
  matrix products  4.98 us (2%)
    pallas_call x1, Pallas kernels, mixer_call(): pl.pallas_call(functools.partial(mixer_kernel, sizes), out_shape=jax.Shap...  136 us
    pallas_call x1, Pallas kernels, front(): pl.pallas_call(functools.partial(front_kernel, (nz, ny, nt, heads, aligne...  101 us
  transfers between devices with their start and end apart: 1, of which 0 were waited for; matrix products, arithmetic and copies ran while one was open for 3% of the time, Pallas kernels for 38%

profile of v2, /device:TPU:0, one launch (start us, length us, event | category | flops | bytes accessed | tf_op | source)
XLA Modules:
  0.0 267.1 jit_solution(7381620783518836039)
XLA Ops:
  6.5 0.0 all-gather.2.cloned.1.call-start
  6.5 0.7 all-gather.2.cloned.1.call-update
  7.3 0.4 copy-done.1
  7.6 0.3 copy.21
  7.9 0.0 copy-done.2
  7.9 0.3 copy.22
  8.2 0.0 copy-done.3
  8.2 0.2 pad_maximum_fusion
  8.5 0.0 copy-start.4
  8.5 0.0 copy-start.5
  8.5 1.5 copy.23
  10.0 0.0 copy-done.4
  10.0 0.2 copy.19
  10.2 0.0 copy-start.9
  10.2 0.2 copy.20
  10.5 0.2 copy.15
  10.7 0.2 copy.16
  10.9 0.1 copy-done.6
  11.0 0.2 copy.17
  11.2 0.2 copy.18
  11.5 0.6 dynamic_slice.5
  12.0 1.2 pad_maximum_fusion.1.qkv
  13.2 1.2 broadcast_in_dim.2.lam_ref
  14.4 100.7 %shard_map.109 = (bf16[16,96,128]{2,1,0:T(8,128)(2,1)}, bf16[1056,2048]{1,0:T(8,128)(2,1)}) custom-call(f32[1,128]{1,0:T(1,128)} %broadcast_in_dim.2.lam_ref, f32[1,128]{1,0:T(1,128)} %bitcast.40, bf16[4,3,384,128]{3,2,1,0:T(8,128)(2,1)} %pad_maximum_fusion.1.qkv, bf16[4,1056,256]{2,1,0:T(8,128)(2,1)} %bitcast.30), custom_call_target="tpu_custom_call" | custom-call | flops 99999997952 | bytes 20000000 | tf_op jit(solution)/shard_map/pallas_call | solution.py:175
  115.1 1.3 copy.26
  116.4 0.3 reshape.37
  116.7 0.0 copy-start.8
  116.7 0.0 all-gather.2.cloned.1.call-done
  116.8 5.0 %multiply_reduce_fusion = (f32[96]{0:T(128)S(1)}, f32[96,2048]{1,0:T(8,128)S(1)}) fusion(bf16[96,2048]{1,0:T(8,128)(2,1)S(1)} %reshape.37, bf16[2048,2048]{1,0:T(8,128)(2,1)} %all-gather.2.cloned.1.call-done, bf16[96,2048]{1,0:T(8,128)(2,1)S(1)} %copy-done.7), kind=kOutput, calls=%fused_computation.4 | convolution fusion | flops 806092672 | bytes 9961856 | tf_op jit(solution)/shard_map/dot_general | solution.py:393
  121.8 1.0 multiply_convert_fusion.normed
  122.8 135.7 %shard_map.110 = bf16[96,2048]{1,0:T(8,128)(2,1)} custom-call(bf16[96,2048]{1,0:T(8,128)(2,1)} %multiply_convert_fusion.normed, f32[96,2048]{1,0:T(8,128)} %copy-done, bf16[1056,2048]{1,0:T(8,128)(2,1)} %get-tuple-element.8.w), custom_call_target="tpu_custom_call" | custom-call | flops 99999997952 | bytes 20000000 | tf_op jit(solution)/shard_map/pallas_call | solution.py:331
  258.5 1.8 copy.28
  (12 shorter events, 0.0 us)
Async XLA Ops:
  6.5 1.1 copy-start.1
  6.5 1.4 copy-start.2
  6.5 1.7 copy-start.3
  6.5 110.2 %all-gather.2.cloned.1.call-start = ((), (), s32[]{:S(2)}) async-start(), calls=%async_computation | async-start | bytes 10485760 | tf_op jit(solution)/shard_map/all_gather | solution.py:380
  8.5 1.5 copy-start.4
  8.5 2.0 copy-start.5
  10.0 1.0 copy-start.6
  10.2 1.2 copy-start.9
  14.4 102.3 %copy-start.7 = (bf16[96,2048]{1,0:T(8,128)(2,1)S(1)}, bf16[96,2048]{1,0:T(8,128)(2,1)}, u32[]{:S(2)}) copy-start(bf16[96,2048]{1,0:T(8,128)(2,1)} %param.11) | copy-start | bytes 1179652
  116.7 5.1 %copy-start.8 = (f32[2048]{0:T(1024)S(1)}, f32[2048]{0:T(1024)}, u32[]{:S(2)}) copy-start(f32[2048]{0:T(1024)} %param.18) | copy-start | bytes 24580
  121.7 1.0 copy-start
Sparse Core Ops, SparseCore 0:
  8.9 62.0 all-gather.1

commit v3 on v2

--- a/solution.py
+++ b/solution.py
@@ -67,13 +67,13 @@
         zp = lax.rem(z + d, nz)
         return remote(place(zp, y), place(zp, y), wy_s.at[d, f], wy_r.at[zp, y], yb=lax.rem(y + f, ny))
 
-    for d in range(1, nz):
+    for d in range(nz - 1, 0, -1):
         q_copy(d).start()
     for f in range(1, ny):
         kv_own(f).start()
     local = pltpu.make_async_copy(w.at[z], place(z, y), l_s)
     local.start()
-    for d in range(1, nz):
+    for d in range(nz - 1, 0, -1):
         w_copy(d).start()
     for f in range(1, ny):
         w_own(f).start()
@@ -133,17 +133,23 @@
             def _():
                 o_copy(p).start()
 
+        @pl.when(i == nz * nt // 2 - 2)
+        def _():
+            w_take(1)
+
         return carry
+
+    def w_take(d):
+        zp = lax.rem(z + d, nz)
+        remote(w.at[z], place(zp, y), w_s.at[d], w_r.at[zp], za=zp).wait_recv()
+        for f in range(1, ny):
+            w_pass(d, f).start()
 
     lax.fori_loop(0, nz * nt // 2, block, 0)
     o_out[me] = osend[me]
-    for d in range(1, nz):
-        zp = lax.rem(z + d, nz)
-        remote(w.at[z], place(zp, y), w_s.at[d], w_r.at[zp], za=zp).wait_recv()
-        if d == 1:
-            local.wait()
-        for f in range(1, ny):
-            w_pass(d, f).start()
+    local.wait()
+    for d in range(2, nz):
+        w_take(d)
     for i in range(1, nz * nt):
         p = lax.rem(me + i, nz * nt)
         remote(osend.at[p], o_out.at[p], o_s.at[p], o_r.at[p], za=p // nt, tp=lax.rem(p, nt)).wait_recv()
@@ -251,7 +257,7 @@
     def rs_z(d):
         return remote(z_send.at[d], z_recv.at[d], rz_s.at[d], rz_r.at[d], za=lax.rem(z + d, nz))
 
-    for d in range(1, nz):
+    for d in range(nz - 1, 0, -1):
         ag_z(d).start()
     for e in range(1, nx):
         ag_x(0, e).start()

time: 267 us -> 249 us (0.933)
  Pallas kernels: 236 us -> 218 us
    pallas_call x1, Pallas kernels: 136 us -> 106 us  [mixer_call(): pl.pallas_call(functools.partial(mixer_kernel, sizes), out_shape=jax.Shap...]
    pallas_call x1, Pallas kernels: 101 us -> 112 us  [front(): pl.pallas_call(functools.partial(front_kernel, (nz, ny, nt, heads, aligne...]
  transfers between devices with their start and end apart: 1 -> 1, of which waited for: 0 -> 0; matrix products, arithmetic and copies ran while one was open for 3% -> 3% of each run, Pallas kernels for 38% -> 45%
where the time goes in v3:
time: 249 us
  Pallas kernels  218 us (88%)
  between operations  13.6 us (5%)
  local copies, waits for them, and re-layouts  9.03 us (4%)
  matrix products  4.98 us (2%)
    pallas_call x1, Pallas kernels, front(): pl.pallas_call(functools.partial(front_kernel, (nz, ny, nt, heads, aligne...  112 us
    pallas_call x1, Pallas kernels, mixer_call(): pl.pallas_call(functools.partial(mixer_kernel, sizes), out_shape=jax.Shap...  106 us
  transfers between devices with their start and end apart: 1, of which 0 were waited for; matrix products, arithmetic and copies ran while one was open for 3% of the time, Pallas kernels for 45%

profile of v3, /device:TPU:0, one launch (start us, length us, event | category | flops | bytes accessed | tf_op | source)
XLA Modules:
  0.0 248.6 jit_solution(6798194314461844565)
XLA Ops:
  6.5 0.0 all-gather.2.cloned.1.call-start
  6.5 0.7 all-gather.2.cloned.1.call-update
  7.3 0.4 copy-done.1
  7.6 0.3 copy.21
  7.9 0.0 copy-done.2
  7.9 0.3 copy.22
  8.2 0.0 copy-done.3
  8.2 0.2 pad_maximum_fusion
  8.5 0.0 copy-start.4
  8.5 0.0 copy-start.5
  8.5 1.5 copy.23
  10.0 0.0 copy-done.4
  10.0 0.2 copy.19
  10.2 0.0 copy-start.9
  10.2 0.2 copy.20
  10.5 0.2 copy.15
  10.7 0.2 copy.16
  10.9 0.1 copy-done.6
  11.0 0.2 copy.17
  11.2 0.2 copy.18
  11.5 0.6 dynamic_slice.5
  12.0 1.2 pad_maximum_fusion.1.qkv
  13.2 1.2 broadcast_in_dim.2.lam_ref
  14.4 111.7 %shard_map.109 = (bf16[16,96,128]{2,1,0:T(8,128)(2,1)}, bf16[1056,2048]{1,0:T(8,128)(2,1)}) custom-call(f32[1,128]{1,0:T(1,128)} %broadcast_in_dim.2.lam_ref, f32[1,128]{1,0:T(1,128)} %bitcast.40, bf16[4,3,384,128]{3,2,1,0:T(8,128)(2,1)} %pad_maximum_fusion.1.qkv, bf16[4,1056,256]{2,1,0:T(8,128)(2,1)} %bitcast.30), custom_call_target="tpu_custom_call" | custom-call | flops 99999997952 | bytes 20000000 | tf_op jit(solution)/shard_map/pallas_call | solution.py:181
  126.2 1.3 copy.26
  127.5 0.3 reshape.37
  127.8 0.0 copy-start.8
  127.8 0.0 all-gather.2.cloned.1.call-done
  127.8 5.0 %multiply_reduce_fusion = (f32[96]{0:T(128)S(1)}, f32[96,2048]{1,0:T(8,128)S(1)}) fusion(bf16[96,2048]{1,0:T(8,128)(2,1)S(1)} %reshape.37, bf16[2048,2048]{1,0:T(8,128)(2,1)} %all-gather.2.cloned.1.call-done, bf16[96,2048]{1,0:T(8,128)(2,1)S(1)} %copy-done.7), kind=kOutput, calls=%fused_computation.4 | convolution fusion | flops 806092672 | bytes 9961856 | tf_op jit(solution)/shard_map/dot_general | solution.py:399
  132.8 1.0 multiply_convert_fusion.normed
  133.8 106.2 %shard_map.110 = bf16[96,2048]{1,0:T(8,128)(2,1)} custom-call(bf16[96,2048]{1,0:T(8,128)(2,1)} %multiply_convert_fusion.normed, f32[96,2048]{1,0:T(8,128)} %copy-done, bf16[1056,2048]{1,0:T(8,128)(2,1)} %get-tuple-element.8.w), custom_call_target="tpu_custom_call" | custom-call | flops 99999997952 | bytes 20000000 | tf_op jit(solution)/shard_map/pallas_call | solution.py:337
  240.0 1.8 copy.28
  (12 shorter events, 0.0 us)
Async XLA Ops:
  6.5 1.1 copy-start.1
  6.5 1.4 copy-start.2
  6.5 1.7 copy-start.3
  6.5 121.3 %all-gather.2.cloned.1.call-start = ((), (), s32[]{:S(2)}) async-start(), calls=%async_computation | async-start | bytes 10485760 | tf_op jit(solution)/shard_map/all_gather | solution.py:386
  8.5 1.5 copy-start.4
  8.5 2.0 copy-start.5
  10.0 1.0 copy-start.6
  10.2 1.2 copy-start.9
  14.4 113.4 %copy-start.7 = (bf16[96,2048]{1,0:T(8,128)(2,1)S(1)}, bf16[96,2048]{1,0:T(8,128)(2,1)}, u32[]{:S(2)}) copy-start(bf16[96,2048]{1,0:T(8,128)(2,1)} %param.11) | copy-start | bytes 1179652
  127.8 5.1 %copy-start.8 = (f32[2048]{0:T(1024)S(1)}, f32[2048]{0:T(1024)}, u32[]{:S(2)}) copy-start(f32[2048]{0:T(1024)} %param.18) | copy-start | bytes 24580
  132.8 1.0 copy-start
Sparse Core Ops, SparseCore 0:
  8.9 63.0 all-gather.1
